TPU v7x, 32 devices: a whole 2x2x4 slice. The times are simulated.
32 devices in a mesh: sp: 8 (over z, y), tp: 4 (over x, core).
Axes of the slice: x: 2, y: 2, z: 4, core: 2. Of those that a mesh axis runs over, the one named last changes fastest.
Arguments:
- tokens: bfloat16 [2560, 2048], P('sp', 'tp'), may hold values from -6 to 6
- pre_gain: float32 [2, 2048], replicated, may hold values from 0.1 to 1.9
- w_value: bfloat16 [2, 2048, 2048], P(None, 'sp', 'tp'), may hold values from -0.125 to 0.125
- w_gate: bfloat16 [2, 2048, 2048], P(None, 'sp', 'tp'), may hold values from -0.125 to 0.125
- taps: float32 [2, 31, 2048], P(None, None, 'tp'), may hold values from -5 to 5
- norm_gain: float32 [2, 2048], P(None, 'tp'), may hold values from 0.1 to 1.9
- norm_shift: float32 [2, 2048], P(None, 'tp'), may hold values from -3 to 3
- w_out: bfloat16 [2, 2048, 2048], P(None, 'tp', 'sp'), may hold values from -2 to 2
- post_gain: float32 [2, 2048], P(None, 'tp'), may hold values from 0.1 to 1.9
Outputs:
- stream: bfloat16 [2560, 2048], P('sp', 'tp')
All inputs are finite; a program needn't handle non-finite values.
Results may differ from a plain program's by a relative error of at most 0.015.
Values may be sent and summed in bfloat16 or wider, within the bound.
A program may use at most 64 MiB of HBM per device.

v0:
```python
import jax
import jax.numpy as jnp
from jax import lax
from jax.sharding import PartitionSpec as P

D = 2048
CONV_WIDTH = 31
LAYERS = 2
EPSILON = 1e-06
LN_EPSILON = 1e-05


def passed_along(block, axis, distance):
    devices = range(lax.axis_size(axis))
    route = [(i - distance, i) for i in devices if i - distance in devices]
    return lax.ppermute(block, axis, route)


def local(tokens, pre_gain, w_value, w_gate, taps, norm_gain, norm_shift, w_out, post_gain):
    stream = tokens
    full_value, full_gate = (
        lax.all_gather(w_value, "sp", axis=1, tiled=True),
        lax.all_gather(w_gate, "sp", axis=1, tiled=True),
    )
    full_out = lax.all_gather(w_out, "sp", axis=2, tiled=True)
    for layer in range(LAYERS):
        whole = lax.all_gather(stream, "tp", axis=1, tiled=True)
        whole_f = whole.astype(jnp.float32)
        normed = (
            whole_f
            * lax.rsqrt(jnp.mean(whole_f * whole_f, -1, keepdims=True) + EPSILON)
            * pre_gain[layer]
        ).astype(jnp.bfloat16)
        value_mat = full_value[layer]
        gate_mat = full_gate[layer]
        out_mat = full_out[layer]
        value_proj = jnp.dot(normed, value_mat, preferred_element_type=jnp.float32)
        gate_proj = jnp.dot(normed, gate_mat, preferred_element_type=jnp.float32)
        glu_act = (value_proj * jax.nn.sigmoid(gate_proj)).astype(jnp.bfloat16)
        rows = glu_act.shape[0]
        fringe = passed_along(glu_act[rows - (CONV_WIDTH - 1) :], "sp", 1)
        padded = jnp.concatenate([fringe, glu_act], 0).astype(jnp.float32)
        conv_out = jnp.zeros(glu_act.shape, jnp.float32)
        for offset in range(CONV_WIDTH):
            conv_out = conv_out + taps[layer, offset] * padded[offset : offset + rows]
        row_sum, row_square = lax.psum(
            (jnp.sum(conv_out, -1, keepdims=True), jnp.sum(conv_out * conv_out, -1, keepdims=True)),
            "tp",
        )
        center = row_sum / D
        spread = jnp.maximum(row_square / D - center * center, 0.0)
        activated = jax.nn.silu(
            (conv_out - center) * lax.rsqrt(spread + LN_EPSILON) * norm_gain[layer]
            + norm_shift[layer]
        ).astype(jnp.bfloat16)
        terms = jnp.dot(activated, out_mat, preferred_element_type=jnp.float32)
        summed = lax.psum_scatter(terms.astype(jnp.bfloat16), "tp", scatter_dimension=1, tiled=True)
        projected = summed.astype(jnp.float32)
        out_square = lax.psum(jnp.sum(projected * projected, -1, keepdims=True), "tp")
        scale = lax.rsqrt(out_square / D + EPSILON)
        stream = (stream.astype(jnp.float32) + projected * scale * post_gain[layer]).astype(
            jnp.bfloat16
        )
    return stream


def solution(mesh):
    placed = (
        P("sp", "tp"),
        P(),
        P(None, "sp", "tp"),
        P(None, "sp", "tp"),
        P(None, None, "tp"),
        P(None, "tp"),
        P(None, "tp"),
        P(None, "tp", "sp"),
        P(None, "tp"),
    )
    return jax.shard_map(
        local, mesh=mesh, in_specs=placed, out_specs=P("sp", "tp"), check_vma=False
    )
```

profile of v0, /device:TPU:0, one launch (start us, length us, event | category | flops | bytes accessed | tf_op | source)
XLA Modules:
  0.0 377.1 jit_solution(16301794310421925368)
XLA Ops:
  6.5 0.7 all-gather.6.cloned.1.call-update
  7.3 0.0 all-gather.10.cloned.1.call-start
  7.3 0.7 all-gather.10.cloned.1.call-update
  8.0 0.0 all-gather.8.cloned.1.call-start
  8.1 0.7 all-gather.8.cloned.1.call-update
  8.7 0.0 all-gather.12.cloned.1.call-start
  8.8 0.5 all-gather.12.cloned.1.call-update
  9.3 0.0 reduce-scatter.3.cloned.1.call-start
  9.4 0.8 fusion.116
  10.1 0.8 fusion.113
  10.9 0.9 fusion.112
  11.8 0.9 fusion.111
  12.7 0.8 fusion.114
  13.5 16.3 %all-gather.6.cloned.1.call-done = bf16[320,2048]{1,0:T(8,128)(2,1)} async-done(((bf16[320,512]{1,0:T(8,128)(2,1)}), bf16[320,2048]{1,0:T(8,128)(2,1)}) %all-gather.6.cloned.1.call-update) | async-done | bytes 1310736 | tf_op jit(solution)/shard_map/all_gather | solution.py:27
  29.8 1.7 fusion
  31.5 73.3 %all-gather.10.cloned.1.call-done = bf16[2,2048,512]{2,1,0:T(8,128)(2,1)} async-done(((bf16[2,256,512]{2,1,0:T(8,128)(2,1)}), bf16[2,2048,512]{2,1,0:T(8,128)(2,1)}) %all-gather.10.cloned.1.call-update) | async-done | bytes 4194320 | tf_op jit(solution)/shard_map/all_gather | solution.py:23
  104.8 3.1 fusion.20
  107.9 70.4 %all-gather.8.cloned.1.call-done = bf16[2,2048,512]{2,1,0:T(8,128)(2,1)} async-done(((bf16[2,256,512]{2,1,0:T(8,128)(2,1)}), bf16[2,2048,512]{2,1,0:T(8,128)(2,1)}) %all-gather.8.cloned.1.call-update) | async-done | bytes 4194320 | tf_op jit(solution)/shard_map/all_gather | solution.py:22
  178.3 2.5 fusion.19
  180.8 2.5 collective-permute-start
  183.3 1.6 collective-permute-done
  184.9 0.1 maximum_convert_fusion
  185.0 3.2 fusion.107
  188.2 6.1 %all-reduce.1 = (f32[320,1]{0,1:T(1,128)S(1)}, f32[320,1]{0,1:T(1,128)S(1)}) all-reduce(f32[320,1]{0,1:T(1,128)S(1)} %broadcast_in_dim.20, f32[320,1]{0,1:T(1,128)S(1)} %broadcast_in_dim.21), channel_id=1, replica_groups=mesh['sp'=8,'tp'=4] {'tp'}, use_global_device_ids=true, to_apply=%region_2.0 | all-reduce | flops 640 | bytes 5120 | tf_op jit(solution)/shard_map/psum | solution.py:46
  194.3 59.2 %all-gather.12.cloned.1.call-done = bf16[2,512,2048]{2,1,0:T(8,128)(2,1)} async-done(((bf16[2,512,256]{2,1,0:T(8,128)(2,1)}), bf16[2,512,2048]{2,1,0:T(8,128)(2,1)}) %all-gather.12.cloned.1.call-update) | async-done | bytes 4194320 | tf_op jit(solution)/shard_map/all_gather | solution.py:25
  253.5 3.8 %convolution_convert_fusion.1 = bf16[320,2048]{1,0:T(8,128)(2,1)} fusion(bf16[2,512,2048]{2,1,0:T(8,128)(2,1)} %all-gather.12.cloned.1.call-done, f32[320,512]{1,0:T(8,128)S(1)} %get-tuple-element.18, f32[512]{0:T(512)S(1)} %bitcast.183, f32[512]{0:T(512)S(1)} %bitcast.182, f32[320]{0:T(512)S(1)} %get-tuple-element.12, f32[320]{0:T(512)S(1)} %get-tuple-element.11), kind=kOutput, calls=%fused_computation.5 | convolution fusion | flops 673218560 | bytes 4069888 | tf_op jit(solution)/shard_map/dot_general | solution.py:56
  257.3 0.0 all-gather.14.cloned.1.call-start
  257.3 24.7 %reduce-scatter.3.cloned.1.call-done = bf16[320,512]{1,0:T(8,128)(2,1)} async-done(((bf16[320,2048]{1,0:T(8,128)(2,1)}), bf16[320,512]{1,0:T(8,128)(2,1)}) %reduce-scatter.3.cloned.1.call-update) | async-done | bytes 327696 | tf_op jit(solution)/shard_map/reduce_scatter | solution.py:57
  282.0 1.1 fusion.22
  283.2 5.8 %psum.44 = f32[320,1]{0,1:T(1,128)S(1)} all-reduce(f32[320,1]{0,1:T(1,128)S(1)} %broadcast_in_dim.22), channel_id=1, replica_groups=mesh['sp'=8,'tp'=4] {'tp'}, use_global_device_ids=true, to_apply=%region_7.8 | all-reduce | flops 320 | bytes 2560 | tf_op jit(solution)/shard_map/psum | solution.py:59
  289.0 1.9 fusion.25
  290.9 0.0 reduce-scatter.5.cloned.1.call-start
  290.9 18.9 %all-gather.14.cloned.1.call-done = bf16[320,2048]{1,0:T(8,128)(2,1)} async-done(((bf16[320,512]{1,0:T(8,128)(2,1)}), bf16[320,2048]{1,0:T(8,128)(2,1)}) %all-gather.14.cloned.1.call-update) | async-done | bytes 1310736 | tf_op jit(solution)/shard_map/all_gather | solution.py:27
  309.8 1.7 fusion.3
  311.5 3.1 fusion.21
  314.6 0.5 copy-done.6
  315.1 0.9 fusion.18
  316.0 3.4 collective-permute-start.1
  319.4 0.9 fusion.110
  320.3 0.7 collective-permute-done.1
  321.0 0.1 maximum_convert_fusion.1
  321.1 3.2 fusion.106
  324.3 6.0 %all-reduce = (f32[320,1]{0,1:T(1,128)S(1)}, f32[320,1]{0,1:T(1,128)S(1)}) all-reduce(f32[320,1]{0,1:T(1,128)S(1)} %broadcast_in_dim.23, f32[320,1]{0,1:T(1,128)S(1)} %broadcast_in_dim.24), channel_id=1, replica_groups=mesh['sp'=8,'tp'=4] {'tp'}, use_global_device_ids=true, to_apply=%region_10.11 | all-reduce | flops 640 | bytes 5120 | tf_op jit(solution)/shard_map/psum | solution.py:46
  330.3 3.7 convolution_convert_fusion
  334.0 27.4 %reduce-scatter.5.cloned.1.call-done = bf16[320,512]{1,0:T(8,128)(2,1)} async-done(((bf16[320,2048]{1,0:T(8,128)(2,1)}), bf16[320,512]{1,0:T(8,128)(2,1)}) %reduce-scatter.5.cloned.1.call-update) | async-done | bytes 327696 | tf_op jit(solution)/shard_map/reduce_scatter | solution.py:57
  361.4 1.1 fusion.26
  362.5 5.8 %psum.47 = f32[320,1]{0,1:T(1,128)S(1)} all-reduce(f32[320,1]{0,1:T(1,128)S(1)} %broadcast_in_dim.25), channel_id=1, replica_groups=mesh['sp'=8,'tp'=4] {'tp'}, use_global_device_ids=true, to_apply=%region_15.16 | all-reduce | flops 320 | bytes 2560 | tf_op jit(solution)/shard_map/psum | solution.py:59
  368.3 1.9 fusion.29
  (33 shorter events, 0.3 us)
Async XLA Ops:
  6.5 23.3 %all-gather.6.cloned.1.call-start = ((), (), s32[]{:S(2)}) async-start(), calls=%async_computation.2 | async-start | bytes 1638400 | tf_op jit(solution)/shard_map/all_gather | solution.py:27
  7.3 97.5 %all-gather.10.cloned.1.call-start = ((), (), s32[]{:S(2)}) async-start(), calls=%async_computation.4 | async-start | bytes 4718592 | tf_op jit(solution)/shard_map/all_gather | solution.py:23
  8.0 170.3 %all-gather.8.cloned.1.call-start = ((), (), s32[]{:S(2)}) async-start(), calls=%async_computation.3 | async-start | bytes 4718592 | tf_op jit(solution)/shard_map/all_gather | solution.py:22
  8.7 244.7 %all-gather.12.cloned.1.call-start = ((), (), s32[]{:S(2)}) async-start(), calls=%async_computation.5 | async-start | bytes 4718592 | tf_op jit(solution)/shard_map/all_gather | solution.py:25
  9.3 272.7 %reduce-scatter.3.cloned.1.call-start = ((), (), s32[]{:S(2)}) async-start(), calls=%async_computation.6 | async-start | bytes 1638400 | tf_op jit(solution)/shard_map/reduce_scatter | solution.py:57
  104.8 73.5 %copy-start.1 = (bf16[320,2048]{1,0:T(8,128)(2,1)S(1)}, bf16[320,2048]{1,0:T(8,128)(2,1)}, u32[]{:S(2)}) copy-start(bf16[320,2048]{1,0:T(8,128)(2,1)} %all-gather.6.cloned.1.call-done) | copy-start | bytes 3932164
  107.9 75.4 %copy-start.4 = (f32[2,512]{1,0:T(2,128)S(1)}, f32[2,512]{1,0:T(2,128)}, u32[]{:S(2)}) copy-start(f32[2,512]{1,0:T(2,128)} %param.15) | copy-start | bytes 12292
  180.8 4.0 %collective-permute-start = (bf16[30,512]{1,0:T(8,128)(2,1)S(1)}, bf16[30,512]{1,0:T(8,128)(2,1)S(1)}, u32[]{:S(2)}, u32[]{:S(2)}) collective-permute-start(bf16[30,512]{1,0:T(8,128)(2,1)S(1)} %slice.562), channel_id=1, source_target_pairs={{0,4},{4,8},{8,12},{12,16},{16,20},{20,24},{24,28},{1,5},{5,9},{9,... | collective-permute-start | bytes 92168 | tf_op jit(solution)/shard_map/ppermute | solution.py:16
  253.4 3.9 %copy-start.5 = (f32[2,512]{1,0:T(2,128)S(1)}, f32[2,512]{1,0:T(2,128)}, u32[]{:S(2)}) copy-start(f32[2,512]{1,0:T(2,128)} %param.17) | copy-start | bytes 12292
  253.4 35.5 %copy-start.3 = (bf16[320,512]{1,0:T(8,128)(2,1)S(1)}, bf16[320,512]{1,0:T(8,128)(2,1)}, u32[]{:S(2)}) copy-start(bf16[320,512]{1,0:T(8,128)(2,1)} %param.9) | copy-start | bytes 983044
  257.3 52.5 %all-gather.14.cloned.1.call-start = ((), (), s32[]{:S(2)}) async-start(), calls=%async_computation.7 | async-start | bytes 1638400 | tf_op jit(solution)/shard_map/all_gather | solution.py:27
  290.9 70.5 %reduce-scatter.5.cloned.1.call-start = ((), (), s32[]{:S(2)}) async-start(), calls=%async_computation.8 | async-start | bytes 1638400 | tf_op jit(solution)/shard_map/reduce_scatter | solution.py:57
  311.5 3.1 copy-start.2
  311.5 3.6 copy-start.6
  316.0 5.0 %collective-permute-start.1 = (bf16[30,512]{1,0:T(8,128)(2,1)S(1)}, bf16[30,512]{1,0:T(8,128)(2,1)S(1)}, u32[]{:S(2)}, u32[]{:S(2)}) collective-permute-start(bf16[30,512]{1,0:T(8,128)(2,1)S(1)} %slice.597), channel_id=1, source_target_pairs={{0,4},{4,8},{8,12},{12,16},{16,20},{20,24},{24,28},{1,5},{5,9},{9,... | collective-permute-start | bytes 92168 | tf_op jit(solution)/shard_map/ppermute | solution.py:16
  330.3 38.1 %copy-start = (bf16[320,512]{1,0:T(8,128)(2,1)S(1)}, bf16[320,512]{1,0:T(8,128)(2,1)}, u32[]{:S(2)}) copy-start(bf16[320,512]{1,0:T(8,128)(2,1)} %fusion.25) | copy-start | bytes 983044
Sparse Core Ops, SparseCore 0:
  8.9 20.8 all-gather.5
  32.0 72.7 all-gather.9
  107.0 71.2 all-gather.7
  180.2 73.1 all-gather.11
  257.4 24.5 reduce-scatter.2
  291.0 18.7 all-gather.13
  334.1 27.2 reduce-scatter.4
where the time goes:
time: 378 us; the launch traced here: 377 us
  waiting for transfers between devices  295 us (78%)
  blocking collectives  23.5 us (6%)
  matrix products  17 us (4%)
  other arithmetic  16 us (4%)
  between operations  13.7 us (4%)
  starting transfers between devices  6.07 us (2%)
  local copies, waits for them, and re-layouts  5.61 us (1%)
    all_gather x1, waiting for transfers between devices, local(): lax.all_gather(w_gate, 'sp', axis=1, tiled=True)  73.3 us
    all_gather x1, waiting for transfers between devices, local(): lax.all_gather(w_value, 'sp', axis=1, tiled=True)  70.4 us
    all_gather x1, waiting for transfers between devices, local(): full_out = lax.all_gather(w_out, 'sp', axis=2, tiled=True)  59.2 us
    reduce_scatter x2, waiting for transfers between devices, local(): lax.psum_scatter(terms.astype(jnp.bfloat16), 'tp', scatter_dimension=1, t...  52.1 us
    all_gather x2, waiting for transfers between devices, local(): whole = lax.all_gather(stream, 'tp', axis=1, tiled=True)  35.2 us
    psum x2, blocking collectives, local(): lax.psum((jnp.sum(conv_out, -1, keepdims=True), jnp.sum(conv_out * conv_o...  12 us
    psum x2, blocking collectives, local(): lax.psum(jnp.sum(projected * projected, -1, keepdims=True), 'tp')  11.5 us
  transfers between devices with their start and end apart: 9, of which 9 were waited for; matrix products, arithmetic and copies ran while one was open for 4% of the time, Pallas kernels for 0%

commit v1 on v0

--- a/solution.py
+++ b/solution.py
@@ -8,6 +8,17 @@
 LAYERS = 2
 EPSILON = 1e-06
 LN_EPSILON = 1e-05
+
+
+def turned_line(array, axis, dim):
+    devices = lax.axis_size(axis)
+    right = [(i, (i + 1) % devices) for i in range(devices)]
+    parts = [array]
+    for reach in range(1, devices):
+        parts = [lax.ppermute(parts[0], axis, right), *parts]
+    whole = jnp.concatenate(parts, axis=dim)
+    shift = (lax.axis_index(axis) + 1) * parts[-1].shape[dim]
+    return jnp.roll(whole, shift, axis=dim)
 
 
 def passed_along(block, axis, distance):
@@ -24,7 +35,7 @@
     )
     full_out = lax.all_gather(w_out, "sp", axis=2, tiled=True)
     for layer in range(LAYERS):
-        whole = lax.all_gather(stream, "tp", axis=1, tiled=True)
+        whole = turned_line(stream, "tp", 1)
         whole_f = whole.astype(jnp.float32)
         normed = (
             whole_f

time: 378 us -> 359 us (0.950)
  waiting for transfers between devices: 295 us -> 274 us
  other arithmetic: 16 us -> 19.9 us
    all_gather x2 -> x0, waiting for transfers between devices: 35.2 us -> none  [local(): whole = lax.all_gather(stream, 'tp', axis=1, tiled=True)]
    ppermute x0 -> x6, waiting for transfers between devices: none -> 35.2 us  [turned_line(): parts = [lax.ppermute(parts[0], axis, right), *parts]]
    all_gather x1, waiting for transfers between devices: 73.3 us -> 51.6 us  [local(): lax.all_gather(w_gate, 'sp', axis=1, tiled=True)]
    reduce_sum x2, other arithmetic: 3.33 us -> 7.93 us  [local(): jnp.mean(whole_f * whole_f, -1, keepdims=True) + EPSILON]
  transfers between devices with their start and end apart: 9 -> 13, of which waited for: 9 -> 13; matrix products, arithmetic and copies ran while one was open for 4% -> 5% of each run, Pallas kernels for 0% -> 0%
where the time goes in v1:
time: 359 us
  waiting for transfers between devices  274 us (76%)
  blocking collectives  23.3 us (6%)
  other arithmetic  19.9 us (6%)
  matrix products  16.2 us (5%)
  between operations  13.4 us (4%)
  starting transfers between devices  7.02 us (2%)
  local copies, waits for them, and re-layouts  5.19 us (1%)
    all_gather x1, waiting for transfers between devices, local(): lax.all_gather(w_value, 'sp', axis=1, tiled=True)  70.9 us
    all_gather x1, waiting for transfers between devices, local(): full_out = lax.all_gather(w_out, 'sp', axis=2, tiled=True)  59.3 us
    reduce_scatter x2, waiting for transfers between devices, local(): lax.psum_scatter(terms.astype(jnp.bfloat16), 'tp', scatter_dimension=1, t...  52.5 us
    all_gather x1, waiting for transfers between devices, local(): lax.all_gather(w_gate, 'sp', axis=1, tiled=True)  51.6 us
    ppermute x6, waiting for transfers between devices, turned_line(): parts = [lax.ppermute(parts[0], axis, right), *parts]  35.2 us
    psum x2, blocking collectives, local(): lax.psum((jnp.sum(conv_out, -1, keepdims=True), jnp.sum(conv_out * conv_o...  11.7 us
    psum x2, blocking collectives, local(): lax.psum(jnp.sum(projected * projected, -1, keepdims=True), 'tp')  11.5 us
    reduce_sum x2, other arithmetic, local(): jnp.mean(whole_f * whole_f, -1, keepdims=True) + EPSILON  7.93 us
  transfers between devices with their start and end apart: 13, of which 13 were waited for; matrix products, arithmetic and copies ran while one was open for 5% of the time, Pallas kernels for 0%

profile of v1, /device:TPU:0, one launch (start us, length us, event | category | flops | bytes accessed | tf_op | source)
XLA Modules:
  0.0 358.5 jit_solution(8951229100149773190)
XLA Ops:
  6.5 0.7 all-gather.6.cloned.1.call-update
  7.3 0.7 all-gather.4.cloned.1.call-update
  8.1 0.7 all-gather.8.cloned.1.call-update
  8.8 0.5 collective-permute-start
  9.3 0.8 fusion.130
  10.1 6.1 %collective-permute-done = bf16[320,512]{1,0:T(8,128)(2,1)S(1)} collective-permute-done((bf16[320,512]{1,0:T(8,128)(2,1)}, bf16[320,512]{1,0:T(8,128)(2,1)S(1)}, u32[]{:S(2)}, u32[]{:S(2)}) %collective-permute-start) | collective-permute-done | bytes 327712 | tf_op jit(solution)/shard_map/ppermute | solution.py:18
  16.3 0.8 fusion.129
  17.0 0.9 fusion.128
  17.9 4.8 %collective-permute-done.1 = bf16[320,512]{1,0:T(8,128)(2,1)S(1)} collective-permute-done((bf16[320,512]{1,0:T(8,128)(2,1)S(1)}, bf16[320,512]{1,0:T(8,128)(2,1)S(1)}, u32[]{:S(2)}, u32[]{:S(2)}) %collective-permute-start.1) | collective-permute-done | bytes 327712 | tf_op jit(solution)/shard_map/ppermute | solution.py:18
  22.7 0.8 fusion.132
  23.5 0.9 fusion.127
  24.4 4.8 %collective-permute-done.2 = bf16[320,512]{1,0:T(8,128)(2,1)S(1)} collective-permute-done((bf16[320,512]{1,0:T(8,128)(2,1)S(1)}, bf16[320,512]{1,0:T(8,128)(2,1)S(1)}, u32[]{:S(2)}, u32[]{:S(2)}) %collective-permute-start.2) | collective-permute-done | bytes 327712 | tf_op jit(solution)/shard_map/ppermute | solution.py:18
  29.2 4.2 %fusion = (f32[320]{0:T(512)S(1)}, bf16[320,2048]{1,0:T(8,128)(2,1)S(1)}) fusion(s32[]{:T(128)S(6)} %select_n.13, bf16[320,512]{1,0:T(8,128)(2,1)} %param.11, bf16[320,512]{1,0:T(8,128)(2,1)S(1)} %collective-permute-done, bf16[320,512]{1,0:T(8,128)(2,1)S(1)} %collective-permute-done.1, bf16[320,512]{1,0:T(8,128)(2,1)S(1)} %collective-permute-done.2), kind=kLoop, calls=%fused_computation.6 | loop fusion | flops 12451520 | bytes 2622724 | tf_op jit(solution)/shard_map/reduce_sum | solution.py:42
  33.5 51.6 %all-gather.6.cloned.1.call-done = bf16[2,2048,512]{2,1,0:T(8,128)(2,1)} async-done(((bf16[2,256,512]{2,1,0:T(8,128)(2,1)}), bf16[2,2048,512]{2,1,0:T(8,128)(2,1)}) %all-gather.6.cloned.1.call-update) | async-done | bytes 4194320 | tf_op jit(solution)/shard_map/all_gather | solution.py:34
  85.0 2.6 fusion.34
  87.7 70.9 %all-gather.4.cloned.1.call-done = bf16[2,2048,512]{2,1,0:T(8,128)(2,1)} async-done(((bf16[2,256,512]{2,1,0:T(8,128)(2,1)}), bf16[2,2048,512]{2,1,0:T(8,128)(2,1)}) %all-gather.4.cloned.1.call-update) | async-done | bytes 4194320 | tf_op jit(solution)/shard_map/all_gather | solution.py:33
  158.6 2.5 fusion.33
  161.1 2.4 collective-permute-start.3
  163.6 1.6 collective-permute-done.3
  165.1 0.1 maximum_convert_fusion
  165.2 3.2 fusion.121
  168.5 6.1 %all-reduce.1 = (f32[320,1]{0,1:T(1,128)S(1)}, f32[320,1]{0,1:T(1,128)S(1)}) all-reduce(f32[320,1]{0,1:T(1,128)S(1)} %broadcast_in_dim.20, f32[320,1]{0,1:T(1,128)S(1)} %broadcast_in_dim.21), channel_id=1, replica_groups=mesh['sp'=8,'tp'=4] {'tp'}, use_global_device_ids=true, to_apply=%region_2.4 | all-reduce | flops 640 | bytes 5120 | tf_op jit(solution)/shard_map/psum | solution.py:57
  174.6 59.3 %all-gather.8.cloned.1.call-done = bf16[2,512,2048]{2,1,0:T(8,128)(2,1)} async-done(((bf16[2,512,256]{2,1,0:T(8,128)(2,1)}), bf16[2,512,2048]{2,1,0:T(8,128)(2,1)}) %all-gather.8.cloned.1.call-update) | async-done | bytes 4194320 | tf_op jit(solution)/shard_map/all_gather | solution.py:36
  233.8 3.8 %convolution_convert_fusion.1 = bf16[320,2048]{1,0:T(8,128)(2,1)} fusion(bf16[2,512,2048]{2,1,0:T(8,128)(2,1)} %all-gather.8.cloned.1.call-done, f32[320,512]{1,0:T(8,128)S(1)} %get-tuple-element.21, f32[512]{0:T(512)S(1)} %bitcast.183, f32[512]{0:T(512)S(1)} %bitcast.182, f32[320]{0:T(512)S(1)} %get-tuple-element.13, f32[320]{0:T(512)S(1)} %get-tuple-element.12), kind=kOutput, calls=%fused_computation.5 | convolution fusion | flops 673218560 | bytes 4069888 | tf_op jit(solution)/shard_map/dot_general | solution.py:67
  237.7 0.0 reduce-scatter.5.cloned.1.call-start
  237.7 24.7 %reduce-scatter.3.cloned.1.call-done = bf16[320,512]{1,0:T(8,128)(2,1)} async-done(((bf16[320,2048]{1,0:T(8,128)(2,1)}), bf16[320,512]{1,0:T(8,128)(2,1)}) %reduce-scatter.3.cloned.1.call-update) | async-done | bytes 327696 | tf_op jit(solution)/shard_map/reduce_scatter | solution.py:68
  262.4 1.1 fusion.36
  263.5 5.8 %psum.44 = f32[320,1]{0,1:T(1,128)S(1)} all-reduce(f32[320,1]{0,1:T(1,128)S(1)} %broadcast_in_dim.22), channel_id=1, replica_groups=mesh['sp'=8,'tp'=4] {'tp'}, use_global_device_ids=true, to_apply=%region_7.9 | all-reduce | flops 320 | bytes 2560 | tf_op jit(solution)/shard_map/psum | solution.py:70
  269.3 1.2 fusion.39
  270.5 0.1 collective-permute-start.4
  270.6 6.5 %collective-permute-done.4 = bf16[320,512]{1,0:T(8,128)(2,1)S(1)} collective-permute-done((bf16[320,512]{1,0:T(8,128)(2,1)S(1)}, bf16[320,512]{1,0:T(8,128)(2,1)S(1)}, u32[]{:S(2)}, u32[]{:S(2)}) %collective-permute-start.4) | collective-permute-done | bytes 327712 | tf_op jit(solution)/shard_map/ppermute | solution.py:18
  277.1 6.5 %collective-permute-done.5 = bf16[320,512]{1,0:T(8,128)(2,1)S(1)} collective-permute-done((bf16[320,512]{1,0:T(8,128)(2,1)S(1)}, bf16[320,512]{1,0:T(8,128)(2,1)S(1)}, u32[]{:S(2)}, u32[]{:S(2)}) %collective-permute-start.5) | collective-permute-done | bytes 327712 | tf_op jit(solution)/shard_map/ppermute | solution.py:18
  283.6 6.5 %collective-permute-done.6 = bf16[320,512]{1,0:T(8,128)(2,1)S(1)} collective-permute-done((bf16[320,512]{1,0:T(8,128)(2,1)S(1)}, bf16[320,512]{1,0:T(8,128)(2,1)S(1)}, u32[]{:S(2)}, u32[]{:S(2)}) %collective-permute-start.6) | collective-permute-done | bytes 327712 | tf_op jit(solution)/shard_map/ppermute | solution.py:18
  290.1 3.7 %fusion.3 = (f32[320]{0:T(512)S(1)}, bf16[320,2048]{1,0:T(8,128)(2,1)S(1)}) fusion(s32[]{:T(128)S(6)} %select_n.13, bf16[320,512]{1,0:T(8,128)(2,1)S(1)} %fusion.39, bf16[320,512]{1,0:T(8,128)(2,1)S(1)} %collective-permute-done.4, bf16[320,512]{1,0:T(8,128)(2,1)S(1)} %collective-permute-done.5, bf16[320,512]{1,0:T(8,128)(2,1)S(1)} %collective-permute-done.6), kind=kLoop, calls=%fused_computation.9 | loop fusion | flops 12451520 | bytes 2622724 | tf_op jit(solution)/shard_map/reduce_sum | solution.py:42
  293.8 2.7 fusion.35
  296.5 0.1 copy-done.3
  296.6 0.9 fusion.32
  297.5 3.8 %collective-permute-start.7 = (bf16[30,512]{1,0:T(8,128)(2,1)S(1)}, bf16[30,512]{1,0:T(8,128)(2,1)S(1)}, u32[]{:S(2)}, u32[]{:S(2)}) collective-permute-start(bf16[30,512]{1,0:T(8,128)(2,1)S(1)} %slice.597), channel_id=1, source_target_pairs={{0,4},{4,8},{8,12},{12,16},{16,20},{20,24},{24,28},{1,5},{5,9},{9,... | collective-permute-start | bytes 92168 | tf_op jit(solution)/shard_map/ppermute | solution.py:27
  301.3 0.9 fusion.126
  302.2 0.5 collective-permute-done.7
  302.7 0.1 maximum_convert_fusion.1
  302.8 3.2 fusion.120
  306.0 5.7 %all-reduce = (f32[320,1]{0,1:T(1,128)S(1)}, f32[320,1]{0,1:T(1,128)S(1)}) all-reduce(f32[320,1]{0,1:T(1,128)S(1)} %broadcast_in_dim.23, f32[320,1]{0,1:T(1,128)S(1)} %broadcast_in_dim.24), channel_id=1, replica_groups=mesh['sp'=8,'tp'=4] {'tp'}, use_global_device_ids=true, to_apply=%region_10.12 | all-reduce | flops 640 | bytes 5120 | tf_op jit(solution)/shard_map/psum | solution.py:57
  311.7 3.7 %convolution_convert_fusion = bf16[320,2048]{1,0:T(8,128)(2,1)} fusion(bf16[2,512,2048]{2,1,0:T(8,128)(2,1)} %all-gather.8.cloned.1.call-done, f32[320,512]{1,0:T(8,128)S(1)} %get-tuple-element.18, f32[512]{0:T(512)S(1)} %bitcast.181, f32[512]{0:T(512)S(1)} %bitcast.180, f32[320]{0:T(512)S(1)} %get-tuple-element.11, f32[320]{0:T(512)S(1)} %get-tuple-element.10), kind=kOutput, calls=%fused_computation.4 | convolution fusion | flops 673218560 | bytes 4069888 | tf_op jit(solution)/shard_map/dot_general | solution.py:67
  315.4 27.8 %reduce-scatter.5.cloned.1.call-done = bf16[320,512]{1,0:T(8,128)(2,1)} async-done(((bf16[320,2048]{1,0:T(8,128)(2,1)}), bf16[320,512]{1,0:T(8,128)(2,1)}) %reduce-scatter.5.cloned.1.call-update) | async-done | bytes 327696 | tf_op jit(solution)/shard_map/reduce_scatter | solution.py:68
  343.2 1.1 fusion.40
  344.3 5.8 %psum.47 = f32[320,1]{0,1:T(1,128)S(1)} all-reduce(f32[320,1]{0,1:T(1,128)S(1)} %broadcast_in_dim.25), channel_id=1, replica_groups=mesh['sp'=8,'tp'=4] {'tp'}, use_global_device_ids=true, to_apply=%region_15.17 | all-reduce | flops 320 | bytes 2560 | tf_op jit(solution)/shard_map/psum | solution.py:70
  350.1 1.9 fusion.43
  (33 shorter events, 0.4 us)
Async XLA Ops:
  6.5 78.5 %all-gather.6.cloned.1.call-start = ((), (), s32[]{:S(2)}) async-start(), calls=%async_computation.3 | async-start | bytes 4718592 | tf_op jit(solution)/shard_map/all_gather | solution.py:34
  7.3 151.3 %all-gather.4.cloned.1.call-start = ((), (), s32[]{:S(2)}) async-start(), calls=%async_computation.2 | async-start | bytes 4718592 | tf_op jit(solution)/shard_map/all_gather | solution.py:33
  8.0 225.8 %all-gather.8.cloned.1.call-start = ((), (), s32[]{:S(2)}) async-start(), calls=%async_computation.4 | async-start | bytes 4718592 | tf_op jit(solution)/shard_map/all_gather | solution.py:36
  8.7 253.7 %reduce-scatter.3.cloned.1.call-start = ((), (), s32[]{:S(2)}) async-start(), calls=%async_computation.5 | async-start | bytes 1638400 | tf_op jit(solution)/shard_map/reduce_scatter | solution.py:68
  8.8 7.4 %collective-permute-start = (bf16[320,512]{1,0:T(8,128)(2,1)}, bf16[320,512]{1,0:T(8,128)(2,1)S(1)}, u32[]{:S(2)}, u32[]{:S(2)}) collective-permute-start(bf16[320,512]{1,0:T(8,128)(2,1)} %param.11), channel_id=1, source_target_pairs={{0,1},{1,2},{2,3},{3,0},{4,5},{5,6},{6,7},{7,4},{8,9},{9,10},{10,1... | collective-permute-start | bytes 983048 | tf_op jit(solution)/shard_map/ppermute | solution.py:18
  16.2 6.5 %collective-permute-start.1 = (bf16[320,512]{1,0:T(8,128)(2,1)S(1)}, bf16[320,512]{1,0:T(8,128)(2,1)S(1)}, u32[]{:S(2)}, u32[]{:S(2)}) collective-permute-start(bf16[320,512]{1,0:T(8,128)(2,1)S(1)} %collective-permute-done), channel_id=1, source_target_pairs={{0,1},{1,2},{2,3},{3,0},{4,5},{5,6},{6,7},{7,4},{8,9},{9,10},{10,1... | collective-permute-start | bytes 983048 | tf_op jit(solution)/shard_map/ppermute | solution.py:18
  22.7 6.5 %collective-permute-start.2 = (bf16[320,512]{1,0:T(8,128)(2,1)S(1)}, bf16[320,512]{1,0:T(8,128)(2,1)S(1)}, u32[]{:S(2)}, u32[]{:S(2)}) collective-permute-start(bf16[320,512]{1,0:T(8,128)(2,1)S(1)} %collective-permute-done.1), channel_id=1, source_target_pairs={{0,1},{1,2},{2,3},{3,0},{4,5},{5,6},{6,7},{7,4},{8,9},{9,10},{10,1... | collective-permute-start | bytes 983048 | tf_op jit(solution)/shard_map/ppermute | solution.py:18
  87.6 75.9 %copy-start.1 = (f32[2,512]{1,0:T(2,128)S(1)}, f32[2,512]{1,0:T(2,128)}, u32[]{:S(2)}) copy-start(f32[2,512]{1,0:T(2,128)} %param.17) | copy-start | bytes 12292
  161.1 4.0 %collective-permute-start.3 = (bf16[30,512]{1,0:T(8,128)(2,1)S(1)}, bf16[30,512]{1,0:T(8,128)(2,1)S(1)}, u32[]{:S(2)}, u32[]{:S(2)}) collective-permute-start(bf16[30,512]{1,0:T(8,128)(2,1)S(1)} %slice.562), channel_id=1, source_target_pairs={{0,4},{4,8},{8,12},{12,16},{16,20},{20,24},{24,28},{1,5},{5,9},{9,... | collective-permute-start | bytes 92168 | tf_op jit(solution)/shard_map/ppermute | solution.py:27
  233.8 3.9 %copy-start.2 = (f32[2,512]{1,0:T(2,128)S(1)}, f32[2,512]{1,0:T(2,128)}, u32[]{:S(2)}) copy-start(f32[2,512]{1,0:T(2,128)} %param.19) | copy-start | bytes 12292
  233.8 35.5 %copy-start = (bf16[320,512]{1,0:T(8,128)(2,1)S(1)}, bf16[320,512]{1,0:T(8,128)(2,1)}, u32[]{:S(2)}) copy-start(bf16[320,512]{1,0:T(8,128)(2,1)} %param.11) | copy-start | bytes 983044
  237.7 105.5 %reduce-scatter.5.cloned.1.call-start = ((), (), s32[]{:S(2)}) async-start(), calls=%async_computation.6 | async-start | bytes 1638400 | tf_op jit(solution)/shard_map/reduce_scatter | solution.py:68
  270.5 6.6 %collective-permute-start.4 = (bf16[320,512]{1,0:T(8,128)(2,1)S(1)}, bf16[320,512]{1,0:T(8,128)(2,1)S(1)}, u32[]{:S(2)}, u32[]{:S(2)}) collective-permute-start(bf16[320,512]{1,0:T(8,128)(2,1)S(1)} %fusion.39), channel_id=1, source_target_pairs={{0,1},{1,2},{2,3},{3,0},{4,5},{5,6},{6,7},{7,4},{8,9},{9,10},{10,1... | collective-permute-start | bytes 983048 | tf_op jit(solution)/shard_map/ppermute | solution.py:18
  277.1 6.5 %collective-permute-start.5 = (bf16[320,512]{1,0:T(8,128)(2,1)S(1)}, bf16[320,512]{1,0:T(8,128)(2,1)S(1)}, u32[]{:S(2)}, u32[]{:S(2)}) collective-permute-start(bf16[320,512]{1,0:T(8,128)(2,1)S(1)} %collective-permute-done.4), channel_id=1, source_target_pairs={{0,1},{1,2},{2,3},{3,0},{4,5},{5,6},{6,7},{7,4},{8,9},{9,10},{10,1... | collective-permute-start | bytes 983048 | tf_op jit(solution)/shard_map/ppermute | solution.py:18
  283.6 6.5 %collective-permute-start.6 = (bf16[320,512]{1,0:T(8,128)(2,1)S(1)}, bf16[320,512]{1,0:T(8,128)(2,1)S(1)}, u32[]{:S(2)}, u32[]{:S(2)}) collective-permute-start(bf16[320,512]{1,0:T(8,128)(2,1)S(1)} %collective-permute-done.5), channel_id=1, source_target_pairs={{0,1},{1,2},{2,3},{3,0},{4,5},{5,6},{6,7},{7,4},{8,9},{9,10},{10,1... | collective-permute-start | bytes 983048 | tf_op jit(solution)/shard_map/ppermute | solution.py:18
  293.8 2.8 copy-start.3
  297.5 5.2 %collective-permute-start.7 = (bf16[30,512]{1,0:T(8,128)(2,1)S(1)}, bf16[30,512]{1,0:T(8,128)(2,1)S(1)}, u32[]{:S(2)}, u32[]{:S(2)}) collective-permute-start(bf16[30,512]{1,0:T(8,128)(2,1)S(1)} %slice.597), channel_id=1, source_target_pairs={{0,4},{4,8},{8,12},{12,16},{16,20},{20,24},{24,28},{1,5},{5,9},{9,... | collective-permute-start | bytes 92168 | tf_op jit(solution)/shard_map/ppermute | solution.py:27
Sparse Core Ops, SparseCore 0:
  9.5 75.4 all-gather.5
  87.2 71.2 all-gather.3
  160.6 73.1 all-gather.7
  237.8 24.5 reduce-scatter.2
  315.5 27.6 reduce-scatter.4
